TPU v7x, 32 devices: a whole 2x2x4 slice. The times are simulated.
32 devices in a mesh: sp: 8 (over z, x), tp: 4 (over y, core).
Axes of the slice: x: 2, y: 2, z: 4, core: 2. Of those that a mesh axis runs over, the one named last changes fastest.
Arguments:
- pool_input: bfloat16 [6144, 1024], P(('sp', 'tp')), may hold values from -6 to 6
- stream_in: bfloat16 [6144, 2048], P(('sp', 'tp')), may hold values from -6 to 6
- group_weight: bfloat16 [4, 256, 256], replicated, may hold values from -0.375 to 0.375
- pool_scale: float32 [1024], replicated, may hold values from 0.1 to 1.9
- out_weight: bfloat16 [1024, 2048], replicated, may hold values from -0.1875 to 0.1875
- norm_gain: float32 [2048], replicated, may hold values from 0.1 to 1.9
- routes: int32 [6144, 2], P(('sp', 'tp')), may hold values from 0 to 31, all different within a row; in each aligned block of 192 rows (0 to 191, 192 to 383, ...) at most 18 rows name the same one
- route_weights: float32 [6144, 2], P(('sp', 'tp')), may hold values from 0.05 to 0.95
- expert_gate: bfloat16 [32, 2048, 1536], P(('sp', 'tp')), may hold values from -0.125 to 0.125
- expert_up: bfloat16 [32, 2048, 1536], P(('sp', 'tp')), may hold values from -0.125 to 0.125
- expert_down: bfloat16 [32, 1536, 2048], P(('sp', 'tp')), may hold values from -0.15625 to 0.15625
Outputs:
- layer_out: bfloat16 [6144, 2048], P(('sp', 'tp'))
Inputs may be any that keep to these rules, and one draw needn't show every extreme that they name: `routes`: each row names two different experts. Within each aligned block of 192 rows (the rows of one device) no expert is named more than 18 times, a bound that some block reaches.
All inputs are finite; a program needn't handle non-finite values.
Results may differ from a plain program's by a relative error of at most 0.011.
Values may be sent and summed in bfloat16 or wider, within the bound.
A program may use at most 128 MiB of HBM per device.

v0:
```python
import jax
import jax.numpy as jnp
from jax import lax
from jax.sharding import PartitionSpec as P

pool_windows = (2, 4, 8, 16)
reach_rows = 15
norm_epsilon = 1e-05


def passed_along(value, axis, steps):
    count = lax.axis_size(axis)
    initial, last = (max(0, -steps), min(count, count - steps))
    return lax.ppermute(value, axis, [(source, source + steps) for source in range(initial, last)])


def apply_expert(arrived, expert_gate, expert_up, expert_down):
    width = arrived.shape[-1]
    inputs = arrived.reshape(-1, width)
    gate = jnp.dot(inputs, expert_gate[0], preferred_element_type=jnp.float32)
    upward = jnp.dot(inputs, expert_up[0], preferred_element_type=jnp.float32)
    hidden = (jax.nn.silu(gate) * upward).astype(jnp.bfloat16)
    result = jnp.dot(hidden, expert_down[0], preferred_element_type=jnp.float32).astype(
        jnp.bfloat16
    )
    return result.reshape(arrived.shape)


def body(
    pool_input,
    stream_in,
    group_weight,
    pool_scale,
    out_weight,
    norm_gain,
    routes,
    route_weights,
    expert_gate,
    expert_up,
    expert_down,
):
    row_count = pool_input.shape[0]
    group_width = pool_input.shape[1] // 4
    width = stream_in.shape[1]
    expert_count = lax.axis_size(("sp", "tp"))
    capacity = max(2, 3 * row_count // expert_count)
    previous = passed_along(pool_input[row_count - reach_rows :], ("sp", "tp"), 1)
    extended = jnp.concatenate([previous, pool_input], axis=0).astype(jnp.float32)
    offset = lax.axis_index(("sp", "tp")) * row_count
    position = (offset + jnp.arange(row_count, dtype=jnp.int32)).astype(jnp.float32)[:, None]
    pieces = []
    for group_index, window in enumerate(pool_windows):
        low = group_index * group_width
        high = low + group_width
        trail = jnp.zeros((row_count, group_width), jnp.float32)
        for lag_step in range(window):
            trail = (
                trail
                + extended[reach_rows - lag_step : reach_rows - lag_step + row_count, low:high]
            )
        count = jnp.minimum(position + 1.0, float(window))
        pooled = (trail / count - extended[reach_rows:, low:high]).astype(jnp.bfloat16)
        mapped = jnp.dot(pooled, group_weight[group_index], preferred_element_type=jnp.float32)
        pieces.append((mapped * pool_scale[low:high]).astype(jnp.bfloat16))
    grouped = jnp.concatenate(pieces, axis=1)
    stream = (
        stream_in.astype(jnp.float32)
        + jnp.dot(grouped, out_weight, preferred_element_type=jnp.float32)
    ).astype(jnp.bfloat16)
    stream_f = stream.astype(jnp.float32)
    scale = lax.rsqrt(jnp.mean(stream_f * stream_f, axis=1, keepdims=True) + norm_epsilon)
    normed = (stream_f * scale * norm_gain).astype(jnp.bfloat16)
    assigned = routes.reshape(-1)
    one_hot = (assigned[:, None] == jnp.arange(expert_count, dtype=jnp.int32)[None, :]).astype(
        jnp.int32
    )
    earlier = jnp.sum((jnp.cumsum(one_hot, axis=0) - one_hot) * one_hot, axis=1)
    slot_index = assigned * capacity + earlier
    owner = jnp.arange(2 * row_count, dtype=jnp.int32) // 2
    slot_rows = jnp.full((expert_count * capacity,), row_count, jnp.int32).at[slot_index].set(owner)
    normed_pad = jnp.concatenate([normed, jnp.zeros((1, width), jnp.bfloat16)], axis=0)
    outgoing = normed_pad[slot_rows].reshape(expert_count, capacity, width)
    answered = apply_expert(
        lax.all_to_all(outgoing, ("sp", "tp"), split_axis=0, concat_axis=0, tiled=True),
        expert_gate,
        expert_up,
        expert_down,
    )
    returned = lax.all_to_all(answered, ("sp", "tp"), split_axis=0, concat_axis=0, tiled=True)
    returned = returned.reshape(expert_count * capacity, width)
    picked = returned[slot_index].reshape(row_count, 2, width)
    combined = (
        stream_f
        + route_weights[:, 0:1] * picked[:, 0].astype(jnp.float32)
        + route_weights[:, 1:2] * picked[:, 1].astype(jnp.float32)
    )
    return combined.astype(jnp.bfloat16)


def solution(mesh):
    placed = (
        P(("sp", "tp"), None),
        P(("sp", "tp"), None),
        P(),
        P(),
        P(),
        P(),
        P(("sp", "tp"), None),
        P(("sp", "tp"), None),
        P(("sp", "tp"), None, None),
        P(("sp", "tp"), None, None),
        P(("sp", "tp"), None, None),
    )
    return jax.shard_map(
        body, mesh=mesh, in_specs=placed, out_specs=P(("sp", "tp"), None), check_vma=False
    )
```

profile of v0, /device:TPU:0, one launch (start us, length us, event | category | flops | bytes accessed | tf_op | source)
XLA Modules:
  0.0 222.6 jit_solution(17448955646799776432)
XLA Ops:
  0.0 0.8 slice.139
  0.8 2.4 %collective-permute-start = (bf16[15,1024]{1,0:T(8,128)(2,1)S(1)}, bf16[15,1024]{1,0:T(8,128)(2,1)S(1)}, u32[]{:S(2)}, u32[]{:S(2)}) collective-permute-start(bf16[15,1024]{1,0:T(8,128)(2,1)S(1)} %slice.139), channel_id=1, source_target_pairs={{0,1},{1,2},{2,3},{3,4},{4,5},{5,6},{6,7},{7,8},{8,9},{9,10},{10,1... | collective-permute-start | bytes 92168 | tf_op jit(solution)/shard_map/ppermute | solution.py:14
  3.2 0.8 copy.13
  4.3 0.7 broadcast_multiply_fusion
  5.0 0.8 fusion.71
  5.9 0.9 reduce-window.6
  6.8 0.2 slice_reduce_fusion
  7.4 2.9 %scatter_custom_fusion = s32[576]{0:T(1024)S(1)} fusion(s32[384]{0:T(512)S(1)} %fusion.63, s32[384]{0:T(512)S(1)} %add_select_fusion, s32[]{:T(128)} %constant.24.clone.1), kind=kCustom, calls=%fused_computation.105 | custom fusion | bytes 2308 | tf_op jit(solution)/shard_map/scatter | solution.py:80
  10.4 1.1 maximum_convert_fusion
  11.5 1.1 fusion.16
  12.7 0.2 fusion.17
  12.9 0.3 fusion.18
  13.2 0.4 fusion.19
  13.7 1.8 copy-done.4
  15.4 0.2 copy-done.5
  15.6 1.2 multiply_reduce_fusion
  16.8 1.1 copy-done
  18.0 0.2 multiply_convert_fusion.1
  18.2 4.0 %gather_fusion = bf16[576,2048]{1,0:T(8,128)(2,1)} fusion(bf16[193,2048]{1,0:T(8,128)(2,1)S(1)} %concatenate.11, s32[1024]{0:T(1024)S(1)} %pad_clamp_fusion.1), kind=kCustom, calls=%fused_computation | custom fusion | bytes 4720896 | tf_op jit(solution)/shard_map/gather | solution.py:82
  22.3 2.7 %reshape.100 = bf16[32,18,2048]{2,1,0:T(8,128)(2,1)S(1)} reshape(bf16[576,2048]{1,0:T(8,128)(2,1)} %gather_fusion) | data formatting | bytes 4718592 | tf_op jit(solution)/shard_map/reshape | solution.py:82
  25.0 78.2 %all_to_all.10 = bf16[32,18,2048]{2,1,0:T(8,128)(2,1)} all-to-all(bf16[32,18,2048]{2,1,0:T(8,128)(2,1)S(1)} %reshape.100), channel_id=1, replica_groups=mesh['sp'=8,'tp'=4] {'sp','tp'}, dimensions={0} | all-to-all | bytes 4718592 | tf_op jit(solution)/shard_map/all_to_all | solution.py:84
  103.2 2.9 %reshape.101 = bf16[576,2048]{1,0:T(8,128)(2,1)S(1)} reshape(bf16[32,18,2048]{2,1,0:T(8,128)(2,1)} %all_to_all.10) | data formatting | bytes 4718592 | tf_op jit(solution)/shard_map/reshape | solution.py:19
  106.1 8.4 %fusion.4 = f32[576,1536]{1,0:T(8,128)} fusion(bf16[576,2048]{1,0:T(8,128)(2,1)S(1)} %reshape.101, bf16[1,2048,1536]{2,1,0:T(8,128)(2,1)} %param.19), kind=kOutput, calls=%fused_computation.7 | convolution fusion | flops 3623878656 | bytes 12189696 | tf_op jit(solution)/shard_map/dot_general | solution.py:20
  114.5 14.7 %fusion.8 = bf16[576,2048]{1,0:T(8,128)(2,1)} fusion(bf16[1,1536,2048]{2,1,0:T(8,128)(2,1)} %param.21, f32[576,1536]{1,0:T(8,128)} %fusion.4, bf16[576,2048]{1,0:T(8,128)(2,1)S(1)} %reshape.101, bf16[1,2048,1536]{2,1,0:T(8,128)(2,1)} %param.20), kind=kOutput, calls=%fused_computation.10 | convolution fusion | flops 7254245376 | bytes 20840448 | tf_op jit(solution)/shard_map/dot_general | solution.py:23
  129.2 4.3 %reshape.102 = bf16[32,18,2048]{2,1,0:T(8,128)(2,1)} reshape(bf16[576,2048]{1,0:T(8,128)(2,1)} %fusion.8) | data formatting | bytes 4718592 | tf_op jit(solution)/shard_map/reshape | solution.py:26
  133.4 3.8 %all-to-all-start.1 = ((bf16[32,18,2048]{2,1,0:T(8,128)(2,1)}), bf16[32,18,2048]{2,1,0:T(8,128)(2,1)}, u32[]{:S(2)}, u32[]{:S(2)}) async-start(bf16[32,18,2048]{2,1,0:T(8,128)(2,1)} %reshape.102), calls=%async_computation.1 | async-start | bytes 6291456 | tf_op jit(solution)/shard_map/all_to_all | solution.py:89
  137.3 71.6 %all-to-all-done.1 = bf16[32,18,2048]{2,1,0:T(8,128)(2,1)} async-done(((bf16[32,18,2048]{2,1,0:T(8,128)(2,1)}), bf16[32,18,2048]{2,1,0:T(8,128)(2,1)}, u32[]{:S(2)}, u32[]{:S(2)}) %all-to-all-start.1) | async-done | bytes 2359328 | tf_op jit(solution)/shard_map/all_to_all | solution.py:89
  208.8 2.9 %reshape.103 = bf16[576,2048]{1,0:T(8,128)(2,1)S(1)} reshape(bf16[32,18,2048]{2,1,0:T(8,128)(2,1)} %all-to-all-done.1) | data formatting | bytes 4718592 | tf_op jit(solution)/shard_map/reshape | solution.py:90
  211.8 3.1 %gather_fusion.1 = bf16[384,2048]{1,0:T(8,128)(2,1)} fusion(bf16[576,2048]{1,0:T(8,128)(2,1)S(1)} %reshape.103, s32[1024]{0:T(1024)S(1)} %pad_clamp_fusion), kind=kCustom, calls=%fused_computation.1 | custom fusion | bytes 3147264 | tf_op jit(solution)/shard_map/gather | solution.py:91
  214.9 2.8 %reshape.104 = bf16[192,2,2048]{2,1,0:T(2,128)(2,1)S(1)} reshape(bf16[384,2048]{1,0:T(8,128)(2,1)} %gather_fusion.1) | data formatting | bytes 3145728 | tf_op jit(solution)/shard_map/reshape | solution.py:91
  217.7 2.2 %fusion.70 = (bf16[192,1,2048]{2,1,0:T(2,128)(2,1)S(1)}, bf16[192,1,2048]{2,1,0:T(2,128)(2,1)S(1)}) fusion(bf16[192,2,2048]{2,1,0:T(2,128)(2,1)S(1)} %reshape.104), kind=kLoop, calls=%fused_computation.118 | loop fusion | bytes 3145728 | tf_op jit(solution)/shard_map/slice | solution.py:94
  220.0 2.6 %fusion.14 = bf16[192,2048]{1,0:T(8,128)(2,1)} fusion(f32[192,2048]{1,0:T(8,128)S(1)} %copy-done.1, bf16[192,1,2048]{2,1,0:T(2,128)(2,1)S(1)} %get-tuple-element.6, bf16[192,1,2048]{2,1,0:T(2,128)(2,1)S(1)} %get-tuple-element.5, f32[192]{0:T(256)S(1)} %bitcast.64, f32[192]{0:T(256)S(1)} %bitcast.63), kind=kLoop, calls=%fused_computation.16 | loop fusion | flops 2752512 | bytes 3933696 | tf_op jit(solution)/shard_map/convert_element_type | solution.py:97
  (29 shorter events, 0.9 us)
Async XLA Ops:
  0.0 12.7 %copy-start.6 = (bf16[4,256,256]{2,1,0:T(8,128)(2,1)S(1)}, bf16[4,256,256]{2,1,0:T(8,128)(2,1)}, u32[]{:S(2)}) copy-start(bf16[4,256,256]{2,1,0:T(8,128)(2,1)} %param.13) | copy-start | bytes 1572868
  0.8 9.6 %collective-permute-start = (bf16[15,1024]{1,0:T(8,128)(2,1)S(1)}, bf16[15,1024]{1,0:T(8,128)(2,1)S(1)}, u32[]{:S(2)}, u32[]{:S(2)}) collective-permute-start(bf16[15,1024]{1,0:T(8,128)(2,1)S(1)} %slice.139), channel_id=1, source_target_pairs={{0,1},{1,2},{2,3},{3,4},{4,5},{5,6},{6,7},{7,8},{8,9},{9,10},{10,1... | collective-permute-start | bytes 92168 | tf_op jit(solution)/shard_map/ppermute | solution.py:14
  13.2 2.2 copy-start.4
  13.2 2.4 %copy-start.5 = (bf16[192,2048]{1,0:T(8,128)(2,1)S(1)}, bf16[192,2048]{1,0:T(8,128)(2,1)}, u32[]{:S(2)}) copy-start(bf16[192,2048]{1,0:T(8,128)(2,1)} %param.12) | copy-start | bytes 2359300
  15.6 2.3 %copy-start.2 = (f32[2048]{0:T(1024)S(1)}, f32[2048]{0:T(1024)}, u32[]{:S(2)}) copy-start(f32[2048]{0:T(1024)} %param.16) | copy-start | bytes 24580
  16.8 1.2 copy-start
  133.4 3.8 %copy-start.3 = (f32[192,2]{0,1:T(2,128)S(1)}, f32[192,2]{0,1:T(2,128)}, u32[]{:S(2)}) copy-start(f32[192,2]{0,1:T(2,128)} %param.18) | copy-start | bytes 4612
  133.4 75.4 %all-to-all-start.1 = ((bf16[32,18,2048]{2,1,0:T(8,128)(2,1)}), bf16[32,18,2048]{2,1,0:T(8,128)(2,1)}, u32[]{:S(2)}, u32[]{:S(2)}) async-start(bf16[32,18,2048]{2,1,0:T(8,128)(2,1)} %reshape.102), calls=%async_computation.1 | async-start | bytes 6291456 | tf_op jit(solution)/shard_map/all_to_all | solution.py:89
  217.7 2.3 %copy-start.1 = (f32[192,2048]{1,0:T(8,128)S(1)}, f32[192,2048]{1,0:T(8,128)}, u32[]{:S(2)}) copy-start(f32[192,2048]{1,0:T(8,128)} %copy-done) | copy-start | bytes 4718596
where the time goes:
time: 223 us
  blocking collectives  78.2 us (35%)
  waiting for transfers between devices  71.6 us (32%)
  local copies, waits for them, and re-layouts  34.4 us (15%)
  matrix products  26.3 us (12%)
  starting transfers between devices  6.19 us (3%)
  other arithmetic  5.7 us (3%)
    all_to_all x1, blocking collectives, body(): lax.all_to_all(outgoing, ('sp', 'tp'), split_axis=0, concat_axis=0, tiled...  78.2 us
    all_to_all x1, waiting for transfers between devices, body(): lax.all_to_all(answered, ('sp', 'tp'), split_axis=0, concat_axis=0, tiled...  71.6 us
    dot_general x1, matrix products, apply_expert(): jnp.dot(hidden, expert_down[0], preferred_element_type=jnp.float32)  14.7 us
    dot_general x1, matrix products, apply_expert(): gate = jnp.dot(inputs, expert_gate[0], preferred_element_type=jnp.float32)  8.36 us
  transfers between devices with their start and end apart: 2, of which 1 were waited for; matrix products, arithmetic and copies ran while one was open for 3% of the time, Pallas kernels for 0%

commit v1 on v0

v1 whole, which is shorter than its diff:
```python
import functools

import jax
import jax.numpy as jnp
from jax import lax
from jax.experimental import pallas as pl
from jax.experimental.pallas import tpu as pltpu
from jax.sharding import PartitionSpec as P

MESH = pl.DeviceIdType.MESH
pool_windows = (2, 4, 8, 16)
halo_rows = 16
norm_epsilon = 1e-05
groups = 4
visit_order = (0, 2, 1, 3)
chunk = 256


def kernel(
    n,
    tp_size,
    main,
    extra,
    pool_hbm,
    stream_hbm,
    group_hbm,
    scale_ref,
    out_hbm,
    gain_ref,
    slot_rows_ref,
    slot_cols_ref,
    route_weights_ref,
    gate_hbm,
    up_hbm,
    down_hbm,
    result_ref,
    pool_buf,
    halo_buf,
    extended,
    stream_buf,
    group_buf,
    outw_buf,
    gate_buf,
    up_buf,
    down_buf,
    normed_buf,
    grouped_buf,
    total,
    hidden_buf,
    sent,
    arrived,
    answer,
    returned,
    sent_x,
    arrived_x,
    answer_x,
    returned_x,
    load_sem,
    halo_send,
    halo_recv,
    own_sem,
    send_sem,
    recv_sem,
):
    f32, bf16 = jnp.float32, jnp.bfloat16
    rows, width = result_ref.shape
    pool_width = pool_buf.shape[1]
    group_width = pool_width // 4
    ff = hidden_buf.shape[1]
    size = n // groups
    per_group = size * (main + extra)
    edge = size * main

    me = lax.axis_index("sp") * tp_size + lax.axis_index("tp")
    my_group = me // size
    my_place = me % size

    def coordinates(device):
        return (device // tp_size, device % tp_size)

    loads = []
    for number, (source, target) in enumerate(
        (
            (pool_hbm, pool_buf),
            (group_hbm, group_buf),
            (out_hbm, outw_buf),
            (stream_hbm, stream_buf),
            (gate_hbm.at[0], gate_buf),
            (up_hbm.at[0], up_buf),
            (down_hbm.at[0], down_buf),
        )
    ):
        copy = pltpu.make_async_copy(source, target, load_sem.at[number])
        copy.start()
        loads.append(copy)

    barrier = pltpu.get_barrier_semaphore()

    def greet(step, carry):
        pl.semaphore_signal(
            barrier, inc=1, device_id=coordinates((me + step) % n), device_id_type=MESH
        )
        return carry

    lax.fori_loop(1, n, greet, 0)
    pl.semaphore_wait(barrier, n - 1)

    halo = pltpu.make_async_remote_copy(
        src_ref=pool_hbm.at[pl.ds(rows - halo_rows, halo_rows)],
        dst_ref=halo_buf,
        send_sem=halo_send,
        recv_sem=halo_recv,
        device_id=coordinates((me + 1) % n),
        device_id_type=MESH,
    )
    halo.start()

    loads[0].wait()
    extended[pl.ds(halo_rows, rows), :] = pool_buf[...].astype(f32)
    loads[1].wait()
    halo.wait()
    extended[pl.ds(0, halo_rows), :] = jnp.where(me > 0, halo_buf[...].astype(f32), 0.0)
    position = (me * rows + lax.broadcasted_iota(jnp.int32, (rows, 1), 0)).astype(f32)
    for index, window in enumerate(pool_windows):
        low = index * group_width
        columns = slice(low, low + group_width)
        own = extended[pl.ds(halo_rows, rows), columns]
        trail = own
        for lag in range(1, window):
            trail = trail + extended[pl.ds(halo_rows - lag, rows), columns]
        count = jnp.minimum(position + 1.0, float(window))
        pooled = (trail / count - own).astype(bf16)
        mapped = jnp.dot(pooled, group_buf[index], preferred_element_type=f32)
        grouped_buf[:, columns] = (mapped * scale_ref[:, columns]).astype(bf16)

    loads[2].wait()
    loads[3].wait()

    def project(step, square):
        columns = pl.ds(pl.multiple_of(step * chunk, chunk), chunk)
        value = stream_buf[:, columns].astype(f32) + jnp.dot(
            grouped_buf[...], outw_buf[:, columns], preferred_element_type=f32
        )
        value = value.astype(bf16).astype(f32)
        total[:, columns] = value
        return square + jnp.sum(value * value, axis=1, keepdims=True)

    square = lax.fori_loop(0, width // chunk, project, jnp.zeros((rows, 1), f32))
    scale = lax.rsqrt(square / width + norm_epsilon)
    normed_buf[...] = (total[...] * scale * gain_ref[...]).astype(bf16)

    def block(buffer, group, place):
        return buffer.at[group, pl.ds(pl.multiple_of(place * main, 16), main)]

    def spread(buffer, buffer_x, group):
        if not extra:
            return
        for place in range(size):
            start = edge + place * extra
            buffer_x[group * size + place] = buffer[group, start : start + extra, :]

    def gather(buffer, buffer_x, group):
        if not extra:
            return
        for place in range(size):
            start = edge + place * extra
            buffer[group, start : start + extra, :] = buffer_x[group * size + place]

    def exchange(way, source, source_x, target, target_x, group, first):
        def one(step, carry):
            place = (my_place + step) % size
            peer = group * size + place
            if main:
                pltpu.make_async_remote_copy(
                    src_ref=block(source, group, place),
                    dst_ref=block(target, my_group, my_place),
                    send_sem=send_sem.at[way, 0, group],
                    recv_sem=recv_sem.at[way, 0, my_group],
                    device_id=coordinates(peer),
                    device_id_type=MESH,
                ).start()
            if extra:
                pltpu.make_async_remote_copy(
                    src_ref=source_x.at[peer],
                    dst_ref=target_x.at[me],
                    send_sem=send_sem.at[way, 1, group],
                    recv_sem=recv_sem.at[way, 1, my_group],
                    device_id=coordinates(peer),
                    device_id_type=MESH,
                ).start()
            return carry

        lax.fori_loop(first, size, one, 0)

    def own_block(way, source, source_x, target, target_x):
        copies = []
        if main:
            copies.append(
                pltpu.make_async_copy(
                    block(source, my_group, my_place),
                    block(target, my_group, my_place),
                    own_sem.at[way, 0],
                )
            )
        if extra:
            copies.append(
                pltpu.make_async_copy(source_x.at[me], target_x.at[me], own_sem.at[way, 1])
            )
        return copies

    def finish(semaphore, way, buffer, buffer_x, group, count):
        if main:
            span = buffer.at[group, pl.ds(0, count * main)]
            pltpu.make_async_copy(span, span, semaphore.at[way, 0, group]).wait()
        if extra:
            span = buffer_x.at[pl.ds(group * size, count)]
            pltpu.make_async_copy(span, span, semaphore.at[way, 1, group]).wait()

    own_out = own_block(0, sent, sent_x, arrived, arrived_x)
    own_back = own_block(1, answer, answer_x, returned, returned_x)

    for turn in visit_order:
        group = (my_group + turn) % groups
        wanted = group * per_group + lax.broadcasted_iota(jnp.int32, (per_group, rows), 0)
        chosen = (wanted == slot_rows_ref[0:1, :]) | (wanted == slot_rows_ref[1:2, :])
        chosen = jnp.where(chosen, 1.0, 0.0).astype(bf16)

        def pick(step, carry, group=group, chosen=chosen):
            columns = pl.ds(pl.multiple_of(step * chunk, chunk), chunk)
            sent[group, :, columns] = jnp.dot(
                chosen, normed_buf[:, columns], preferred_element_type=f32
            ).astype(bf16)
            return carry

        lax.fori_loop(0, width // chunk, pick, 0)
        spread(sent, sent_x, group)
        exchange(0, sent, sent_x, arrived, arrived_x, group, 1 if turn == 0 else 0)
        if turn == 0:
            for copy in own_out:
                copy.start()

    for copy in loads[4:]:
        copy.wait()

    for turn in visit_order:
        group = (my_group + groups - turn) % groups
        finish(recv_sem, 0, arrived, arrived_x, group, size - 1 if turn == 0 else size)
        if turn == 0:
            for copy in own_out:
                copy.wait()
        gather(arrived, arrived_x, group)

        def hide(step, carry, group=group):
            columns = pl.ds(pl.multiple_of(step * chunk, chunk), chunk)
            inputs = arrived[group]
            gate = jnp.dot(inputs, gate_buf[:, columns], preferred_element_type=f32)
            upward = jnp.dot(inputs, up_buf[:, columns], preferred_element_type=f32)
            hidden_buf[:, columns] = (gate / (1.0 + jnp.exp(-gate)) * upward).astype(bf16)
            return carry

        lax.fori_loop(0, ff // chunk, hide, 0)

        def lower(step, carry, group=group):
            columns = pl.ds(pl.multiple_of(step * chunk, chunk), chunk)
            answer[group, :, columns] = jnp.dot(
                hidden_buf[...], down_buf[:, columns], preferred_element_type=f32
            ).astype(bf16)
            return carry

        lax.fori_loop(0, width // chunk, lower, 0)
        spread(answer, answer_x, group)
        exchange(1, answer, answer_x, returned, returned_x, group, 1 if turn == 0 else 0)
        if turn == 0:
            for copy in own_back:
                copy.start()

    for turn in visit_order:
        group = (my_group + turn) % groups
        finish(recv_sem, 1, returned, returned_x, group, size - 1 if turn == 0 else size)
        if turn == 0:
            for copy in own_back:
                copy.wait()
        gather(returned, returned_x, group)
        offered = group * per_group + lax.broadcasted_iota(jnp.int32, (rows, per_group), 1)
        mix = jnp.where(offered == slot_cols_ref[:, 0:1], route_weights_ref[:, 0:1], 0.0)
        mix = mix + jnp.where(offered == slot_cols_ref[:, 1:2], route_weights_ref[:, 1:2], 0.0)
        high = mix.astype(bf16)
        rest = (mix - high.astype(f32)).astype(bf16)

        def combine(step, carry, group=group, high=high, rest=rest, last=turn == visit_order[-1]):
            columns = pl.ds(pl.multiple_of(step * chunk, chunk), chunk)
            value = returned[group, :, columns]
            value = (
                total[:, columns]
                + jnp.dot(high, value, preferred_element_type=f32)
                + jnp.dot(rest, value, preferred_element_type=f32)
            )
            if last:
                result_ref[:, columns] = value.astype(bf16)
            else:
                total[:, columns] = value
            return carry

        lax.fori_loop(0, width // chunk, combine, 0)

    for turn in visit_order:
        count = size - 1 if turn == 0 else size
        finish(send_sem, 0, sent, sent_x, (my_group + turn) % groups, count)
        finish(send_sem, 1, answer, answer_x, (my_group + groups - turn) % groups, count)


def body(
    pool_input,
    stream_in,
    group_weight,
    pool_scale,
    out_weight,
    norm_gain,
    routes,
    route_weights,
    expert_gate,
    expert_up,
    expert_down,
):
    rows, pool_width = pool_input.shape
    width = stream_in.shape[1]
    ff = expert_gate.shape[2]
    n = lax.axis_size(("sp", "tp"))
    tp_size = lax.axis_size("tp")
    capacity = max(2, 3 * rows // n)
    main = capacity // 16 * 16
    extra = capacity - main
    size = n // groups
    per_group = size * capacity

    assigned = routes.T.reshape(-1)
    count = assigned.shape[0]
    order = jnp.arange(count, dtype=jnp.int32)
    same = (assigned[:, None] == assigned[None, :]) & (order[:, None] > order[None, :])
    earlier = jnp.sum(same.astype(jnp.int32), axis=1)
    place = assigned % size
    slot = (assigned // size) * per_group + jnp.where(
        earlier < main,
        place * main + earlier,
        size * main + place * extra + earlier - main,
    )
    slot_rows = slot.reshape(2, rows)

    bf16, f32 = jnp.bfloat16, jnp.float32
    vmem = pl.BlockSpec(memory_space=pltpu.VMEM)
    anywhere = pl.BlockSpec(memory_space=pl.ANY)
    slots = pltpu.VMEM((groups, per_group, width), bf16)
    slots_x = pltpu.VMEM((n, max(extra, 1), width), bf16)
    return pl.pallas_call(
        functools.partial(kernel, n, tp_size, main, extra),
        out_shape=jax.ShapeDtypeStruct((rows, width), bf16),
        in_specs=[
            anywhere,
            anywhere,
            anywhere,
            vmem,
            anywhere,
            vmem,
            vmem,
            vmem,
            vmem,
            anywhere,
            anywhere,
            anywhere,
        ],
        out_specs=vmem,
        scratch_shapes=[
            pltpu.VMEM((rows, pool_width), bf16),
            pltpu.VMEM((halo_rows, pool_width), bf16),
            pltpu.VMEM((halo_rows + rows, pool_width), f32),
            pltpu.VMEM((rows, width), bf16),
            pltpu.VMEM(group_weight.shape, bf16),
            pltpu.VMEM(out_weight.shape, bf16),
            pltpu.VMEM(expert_gate.shape[1:], bf16),
            pltpu.VMEM(expert_up.shape[1:], bf16),
            pltpu.VMEM(expert_down.shape[1:], bf16),
            pltpu.VMEM((rows, width), bf16),
            pltpu.VMEM((rows, pool_width), bf16),
            pltpu.VMEM((rows, width), f32),
            pltpu.VMEM((per_group, ff), bf16),
            slots,
            slots,
            slots,
            slots,
            slots_x,
            slots_x,
            slots_x,
            slots_x,
            pltpu.SemaphoreType.DMA((7,)),
            pltpu.SemaphoreType.DMA,
            pltpu.SemaphoreType.DMA,
            pltpu.SemaphoreType.DMA((2, 2)),
            pltpu.SemaphoreType.DMA((2, 2, groups)),
            pltpu.SemaphoreType.DMA((2, 2, groups)),
        ],
        compiler_params=pltpu.CompilerParams(
            collective_id=0, has_side_effects=True, vmem_limit_bytes=60 * 1024 * 1024
        ),
    )(
        pool_input,
        stream_in,
        group_weight,
        pool_scale[None, :],
        out_weight,
        norm_gain[None, :],
        slot_rows,
        slot_rows.T,
        route_weights,
        expert_gate,
        expert_up,
        expert_down,
    )


def solution(mesh):
    placed = (
        P(("sp", "tp"), None),
        P(("sp", "tp"), None),
        P(),
        P(),
        P(),
        P(),
        P(("sp", "tp"), None),
        P(("sp", "tp"), None),
        P(("sp", "tp"), None, None),
        P(("sp", "tp"), None, None),
        P(("sp", "tp"), None, None),
    )
    return jax.shard_map(
        body, mesh=mesh, in_specs=placed, out_specs=P(("sp", "tp"), None), check_vma=False
    )
```

time: 223 us -> 128 us (0.57)
  the two profiles are of different devices: /device:TPU:0 before, /device:TPU:13 now
where the time goes in v1:
time: 128 us
  Pallas kernels  122 us (95%)
  local copies, waits for them, and re-layouts  5.37 us (4%)
    pallas_call x1, Pallas kernels, body(): pl.pallas_call(functools.partial(kernel, n, tp_size, main, extra), out_sh...  122 us
    unnamed x5, local copies, waits for them, and re-layouts  4.32 us

profile of v1, /device:TPU:13, one launch (start us, length us, event | category | flops | bytes accessed | tf_op | source)
XLA Modules:
  0.0 127.9 jit_solution(6090257979114980039)
XLA Ops:
  0.0 0.8 copy.22
  0.8 0.1 copy.23
  0.9 0.1 eq.17
  1.0 0.2 convert_reduce_fusion
  1.2 0.1 reduce_sum.12
  1.3 0.1 copy.24
  1.4 0.1 fusion.2
  1.6 0.0 copy-start
  1.6 0.7 copy.27.slot_rows_ref
  2.2 1.4 %copy.28.route_weights_ref = f32[192,2]{1,0:T(8,128)} copy(f32[192,2]{0,1:T(2,128)} %param.18) | data formatting | bytes 3072 | tf_op args[7]
  3.7 0.0 copy-done
  3.7 122.1 %shard_map.109 = bf16[192,2048]{1,0:T(8,128)(2,1)} custom-call(bf16[192,1024]{1,0:T(8,128)(2,1)} %pool_hbm.1, bf16[192,2048]{1,0:T(8,128)(2,1)} %stream_hbm.1, bf16[4,256,256]{2,1,0:T(8,128)(2,1)} %group_hbm.1, f32[1,1024]{1,0:T(1,128)} %bitcast.8, bf16[1024,2048]{1,0:T(8,128)(2,1)} %out_hbm.1, f32[1,2048]{1,0:T(1,128)} %bitcast.7, ...), custom_call_target="tpu_custom_call" | custom-call | tf_op jit(solution)/shard_map/pallas_call | solution.py:354
  125.8 2.1 %copy.30 = bf16[192,2048]{1,0:T(8,128)(2,1)} copy(bf16[192,2048]{1,0:T(8,128)(2,1)} %shard_map.109) | data formatting | bytes 1572864
Async XLA Ops:
  1.6 2.1 %copy-start = (s32[2,192]{0,1:T(8,128)}, s32[2,192]{0,1:T(8,128)S(1)}, u32[]{:S(2)}) copy-start(s32[2,192]{0,1:T(8,128)S(1)} %fusion.2) | copy-start | bytes 4612

commit v2 on v1

v2 whole, which is shorter than its diff:
```python
import functools

import jax
import jax.numpy as jnp
from jax import lax
from jax.experimental import pallas as pl
from jax.experimental.pallas import tpu as pltpu
from jax.sharding import PartitionSpec as P

MESH = pl.DeviceIdType.MESH
pool_windows = (2, 4, 8, 16)
halo_rows = 16
norm_epsilon = 1e-05
halves = 2
parts = 4
chunk = 256


def kernel(
    n,
    tp_size,
    main,
    extra,
    pool_hbm,
    stream_hbm,
    group_hbm,
    scale_ref,
    out_hbm,
    gain_ref,
    table_ref,
    gate_hbm,
    up_hbm,
    down_hbm,
    result_ref,
    pool_buf,
    halo_buf,
    extended,
    stream_buf,
    group_buf,
    outw_buf,
    gate_buf,
    up_buf,
    down_buf,
    normed_buf,
    grouped_buf,
    total,
    hidden_buf,
    sent,
    arrived,
    answer,
    returned,
    sent_x,
    arrived_x,
    answer_x,
    returned_x,
    raw_buf,
    mixed_buf,
    came_buf,
    far_table,
    load_sem,
    table_send,
    table_recv,
    mirror_send,
    mirror_recv,
    halo_send,
    halo_recv,
    own_sem,
    send_sem,
    recv_sem,
):
    f32, bf16 = jnp.float32, jnp.bfloat16
    rows, width = result_ref.shape
    pool_width = pool_buf.shape[1]
    group_width = pool_width // 4
    ff = hidden_buf.shape[1]
    size = n // halves
    per_half = size * (main + extra)
    edge = size * main

    me = lax.axis_index("sp") * tp_size + lax.axis_index("tp")
    my_half = me // size
    my_place = me % size

    def coordinates(device):
        return (device // tp_size, device % tp_size)

    mirror = coordinates((me + size) % n)

    loads = []
    for number, (source, target) in enumerate(
        (
            (pool_hbm, pool_buf),
            (group_hbm, group_buf),
            (out_hbm, outw_buf),
            (stream_hbm, stream_buf),
            (gate_hbm.at[0], gate_buf),
            (up_hbm.at[0], up_buf),
            (down_hbm.at[0], down_buf),
        )
    ):
        copy = pltpu.make_async_copy(source, target, load_sem.at[number])
        copy.start()
        loads.append(copy)

    barrier = pltpu.get_barrier_semaphore()

    def greet(step, carry):
        pl.semaphore_signal(
            barrier, inc=1, device_id=coordinates((me + step) % n), device_id_type=MESH
        )
        return carry

    lax.fori_loop(1, n, greet, 0)
    pl.semaphore_wait(barrier, n - 1)

    halo = pltpu.make_async_remote_copy(
        src_ref=pool_hbm.at[pl.ds(rows - halo_rows, halo_rows)],
        dst_ref=halo_buf,
        send_sem=halo_send,
        recv_sem=halo_recv,
        device_id=coordinates((me + 1) % n),
        device_id_type=MESH,
    )
    halo.start()
    table_copy = pltpu.make_async_remote_copy(
        src_ref=table_ref,
        dst_ref=far_table,
        send_sem=table_send,
        recv_sem=table_recv,
        device_id=mirror,
        device_id_type=MESH,
    )
    table_copy.start()

    loads[0].wait()
    extended[pl.ds(halo_rows, rows), :] = pool_buf[...].astype(f32)
    loads[1].wait()
    halo.wait()
    extended[pl.ds(0, halo_rows), :] = jnp.where(me > 0, halo_buf[...].astype(f32), 0.0)
    position = (me * rows + lax.broadcasted_iota(jnp.int32, (rows, 1), 0)).astype(f32)
    for index, window in enumerate(pool_windows):
        low = index * group_width
        columns = slice(low, low + group_width)
        own = extended[pl.ds(halo_rows, rows), columns]
        trail = own
        for lag in range(1, window):
            trail = trail + extended[pl.ds(halo_rows - lag, rows), columns]
        count = jnp.minimum(position + 1.0, float(window))
        pooled = (trail / count - own).astype(bf16)
        mapped = jnp.dot(pooled, group_buf[index], preferred_element_type=f32)
        grouped_buf[:, columns] = (mapped * scale_ref[:, columns]).astype(bf16)

    loads[2].wait()
    loads[3].wait()

    def project(step, square):
        columns = pl.ds(pl.multiple_of(step * chunk, chunk), chunk)
        value = stream_buf[:, columns].astype(f32) + jnp.dot(
            grouped_buf[...], outw_buf[:, columns], preferred_element_type=f32
        )
        value = value.astype(bf16).astype(f32)
        total[:, columns] = value
        return square + jnp.sum(value * value, axis=1, keepdims=True)

    square = lax.fori_loop(0, width // chunk, project, jnp.zeros((rows, 1), f32))
    scale = lax.rsqrt(square / width + norm_epsilon)
    normed_buf[...] = (total[...] * scale * gain_ref[...]).astype(bf16)

    def block(buffer, part, place, columns):
        return buffer.at[part, pl.ds(pl.multiple_of(place * main, 16), main), columns]

    def spread(buffer, buffer_x, part, columns):
        if extra:
            for place in range(size):
                start = edge + place * extra
                buffer_x[part, place, :, columns] = buffer[part, start : start + extra, columns]

    def gather(buffer, buffer_x, part, columns):
        if extra:
            for place in range(size):
                start = edge + place * extra
                buffer[part, start : start + extra, columns] = buffer_x[part, place, :, columns]

    def own_copies(way, source, source_x, target, target_x, part, columns, number):
        copies = []
        if main:
            copies.append(
                pltpu.make_async_copy(
                    block(source, part, my_place, columns),
                    block(target, part, my_place, columns),
                    own_sem.at[way, 0, number],
                )
            )
        if extra:
            copies.append(
                pltpu.make_async_copy(
                    source_x.at[part, my_place, :, columns],
                    target_x.at[part, my_place, :, columns],
                    own_sem.at[way, 1, number],
                )
            )
        return copies

    def exchange(way, source, source_x, target, target_x, part, columns, number):
        spread(source, source_x, part, columns)

        def one(step, carry):
            place = (my_place + step) % size
            peer = coordinates(my_half * size + place)
            if main:
                pltpu.make_async_remote_copy(
                    src_ref=block(source, part, place, columns),
                    dst_ref=block(target, part, my_place, columns),
                    send_sem=send_sem.at[way, 0, number],
                    recv_sem=recv_sem.at[way, 0, number],
                    device_id=peer,
                    device_id_type=MESH,
                ).start()
            if extra:
                pltpu.make_async_remote_copy(
                    src_ref=source_x.at[part, place, :, columns],
                    dst_ref=target_x.at[part, my_place, :, columns],
                    send_sem=send_sem.at[way, 1, number],
                    recv_sem=recv_sem.at[way, 1, number],
                    device_id=peer,
                    device_id_type=MESH,
                ).start()
            return carry

        lax.fori_loop(1, size, one, 0)
        for copy in own_copies(way, source, source_x, target, target_x, part, columns, number):
            copy.start()

    def finish(semaphore, way, buffer, buffer_x, part, columns, number):
        if main:
            span = buffer.at[part, pl.ds(0, (size - 1) * main), columns]
            pltpu.make_async_copy(span, span, semaphore.at[way, 0, number]).wait()
        if extra:
            span = buffer_x.at[part, pl.ds(0, size - 1), :, columns]
            pltpu.make_async_copy(span, span, semaphore.at[way, 1, number]).wait()

    def receive(way, source, source_x, target, target_x, part, columns, number):
        finish(recv_sem, way, target, target_x, part, columns, number)
        for copy in own_copies(way, source, source_x, target, target_x, part, columns, number):
            copy.wait()
        gather(target, target_x, part, columns)

    def to_mirror(source, target, number, columns):
        return pltpu.make_async_remote_copy(
            src_ref=source.at[:, columns],
            dst_ref=target.at[:, columns],
            send_sem=mirror_send.at[number],
            recv_sem=mirror_recv.at[number],
            device_id=mirror,
            device_id_type=MESH,
        )

    whole = slice(0, width)
    part_width = width // parts
    pieces = [slice(c * part_width, (c + 1) * part_width) for c in range(parts)]
    out_raw = [to_mirror(normed_buf, raw_buf, c, pieces[c]) for c in range(parts)]
    out_sum = [to_mirror(mixed_buf, came_buf, parts + c, pieces[c]) for c in range(parts)]

    base = my_half * per_half
    wanted = (base + lax.broadcasted_iota(jnp.int32, (per_half, rows), 0)).astype(f32)

    def chosen(table):
        hit = (wanted == table[0:1, :]) | (wanted == table[1:2, :])
        return jnp.where(hit, 1.0, 0.0).astype(bf16)

    def mixing(table):
        mix = jnp.where(wanted == table[0:1, :], table[2:3, :], 0.0)
        mix = mix + jnp.where(wanted == table[1:2, :], table[3:4, :], 0.0)
        high = mix.astype(bf16)
        return high, (mix - high.astype(f32)).astype(bf16)

    def weigh(mix, value):
        dims = (((0,), (0,)), ((), ()))
        first = lax.dot_general(mix[0], value, dims, preferred_element_type=f32)
        return first + lax.dot_general(mix[1], value, dims, preferred_element_type=f32)

    def hide(part):
        def one(step, carry):
            columns = pl.ds(pl.multiple_of(step * chunk, chunk), chunk)
            inputs = arrived[part]
            gate = jnp.dot(inputs, gate_buf[:, columns], preferred_element_type=f32)
            upward = jnp.dot(inputs, up_buf[:, columns], preferred_element_type=f32)
            hidden_buf[:, columns] = (gate / (1.0 + jnp.exp(-gate)) * upward).astype(bf16)
            return carry

        lax.fori_loop(0, ff // chunk, one, 0)

    there = (sent, sent_x, arrived, arrived_x)
    back = (answer, answer_x, returned, returned_x)

    own_chosen = chosen(table_ref)
    for columns in pieces:
        sent[0, :, columns] = jnp.dot(
            own_chosen, normed_buf[:, columns], preferred_element_type=f32
        ).astype(bf16)
    exchange(0, *there, 0, whole, 0)
    for copy in out_raw:
        copy.start()

    table_copy.wait()
    far_chosen = chosen(far_table)

    def serve_own():
        for copy in loads[4:]:
            copy.wait()
        receive(0, *there, 0, whole, 0)
        hide(0)
        for columns in pieces:
            answer[0, :, columns] = jnp.dot(
                hidden_buf[...], down_buf[:, columns], preferred_element_type=f32
            ).astype(bf16)
        exchange(1, *back, 0, whole, 0)

    for c, columns in enumerate(pieces):
        out_raw[c].wait_recv()
        sent[1, :, columns] = jnp.dot(
            far_chosen, raw_buf[:, columns], preferred_element_type=f32
        ).astype(bf16)
        exchange(0, *there, 1, columns, 1 + c)
        if c == parts - 1:
            serve_own()

    for c, columns in enumerate(pieces):
        receive(0, *there, 1, columns, 1 + c)
    hide(1)
    for c, columns in enumerate(pieces):
        answer[1, :, columns] = jnp.dot(
            hidden_buf[...], down_buf[:, columns], preferred_element_type=f32
        ).astype(bf16)
        exchange(1, *back, 1, columns, 1 + c)

    far_mix = mixing(far_table)
    for c, columns in enumerate(pieces):
        receive(1, *back, 1, columns, 1 + c)
        mixed_buf[:, columns] = weigh(far_mix, returned[1, :, columns]).astype(bf16)
        out_sum[c].start()

    receive(1, *back, 0, whole, 0)
    own_mix = mixing(table_ref)
    for columns in pieces:
        total[:, columns] = total[:, columns] + weigh(own_mix, returned[0, :, columns])

    for c, columns in enumerate(pieces):
        out_sum[c].wait_recv()
        result_ref[:, columns] = (total[:, columns] + came_buf[:, columns].astype(f32)).astype(bf16)

    for c in range(parts):
        out_raw[c].wait_send()
        out_sum[c].wait_send()
    for way, source, source_x in ((0, sent, sent_x), (1, answer, answer_x)):
        finish(send_sem, way, source, source_x, 0, whole, 0)
        for c, columns in enumerate(pieces):
            finish(send_sem, way, source, source_x, 1, columns, 1 + c)


def body(
    pool_input,
    stream_in,
    group_weight,
    pool_scale,
    out_weight,
    norm_gain,
    routes,
    route_weights,
    expert_gate,
    expert_up,
    expert_down,
):
    rows, pool_width = pool_input.shape
    width = stream_in.shape[1]
    ff = expert_gate.shape[2]
    n = lax.axis_size(("sp", "tp"))
    tp_size = lax.axis_size("tp")
    capacity = max(2, 3 * rows // n)
    main = capacity // 16 * 16
    extra = capacity - main
    size = n // halves
    per_half = size * capacity

    assigned = routes.T.reshape(-1)
    count = assigned.shape[0]
    order = jnp.arange(count, dtype=jnp.int32)
    same = (assigned[:, None] == assigned[None, :]) & (order[:, None] > order[None, :])
    earlier = jnp.sum(same.astype(jnp.int32), axis=1)
    place = assigned % size
    slot = (assigned // size) * per_half + jnp.where(
        earlier < main,
        place * main + earlier,
        size * main + place * extra + earlier - main,
    )
    table = jnp.concatenate(
        [
            slot.reshape(2, rows).astype(jnp.float32),
            route_weights.T,
            jnp.zeros((4, rows), jnp.float32),
        ]
    )

    bf16, f32 = jnp.bfloat16, jnp.float32
    vmem = pl.BlockSpec(memory_space=pltpu.VMEM)
    anywhere = pl.BlockSpec(memory_space=pl.ANY)
    slots = pltpu.VMEM((halves, per_half, width), bf16)
    slots_x = pltpu.VMEM((halves, size, max(extra, 1), width), bf16)
    return pl.pallas_call(
        functools.partial(kernel, n, tp_size, main, extra),
        out_shape=jax.ShapeDtypeStruct((rows, width), bf16),
        in_specs=[
            anywhere,
            anywhere,
            anywhere,
            vmem,
            anywhere,
            vmem,
            vmem,
            anywhere,
            anywhere,
            anywhere,
        ],
        out_specs=vmem,
        scratch_shapes=[
            pltpu.VMEM((rows, pool_width), bf16),
            pltpu.VMEM((halo_rows, pool_width), bf16),
            pltpu.VMEM((halo_rows + rows, pool_width), f32),
            pltpu.VMEM((rows, width), bf16),
            pltpu.VMEM(group_weight.shape, bf16),
            pltpu.VMEM(out_weight.shape, bf16),
            pltpu.VMEM(expert_gate.shape[1:], bf16),
            pltpu.VMEM(expert_up.shape[1:], bf16),
            pltpu.VMEM(expert_down.shape[1:], bf16),
            pltpu.VMEM((rows, width), bf16),
            pltpu.VMEM((rows, pool_width), bf16),
            pltpu.VMEM((rows, width), f32),
            pltpu.VMEM((per_half, ff), bf16),
            slots,
            slots,
            slots,
            slots,
            slots_x,
            slots_x,
            slots_x,
            slots_x,
            pltpu.VMEM((rows, width), bf16),
            pltpu.VMEM((rows, width), bf16),
            pltpu.VMEM((rows, width), bf16),
            pltpu.VMEM((8, rows), f32),
            pltpu.SemaphoreType.DMA((7,)),
            pltpu.SemaphoreType.DMA,
            pltpu.SemaphoreType.DMA,
            pltpu.SemaphoreType.DMA((2 * parts,)),
            pltpu.SemaphoreType.DMA((2 * parts,)),
            pltpu.SemaphoreType.DMA,
            pltpu.SemaphoreType.DMA,
            pltpu.SemaphoreType.DMA((2, 2, 1 + parts)),
            pltpu.SemaphoreType.DMA((2, 2, 1 + parts)),
            pltpu.SemaphoreType.DMA((2, 2, 1 + parts)),
        ],
        compiler_params=pltpu.CompilerParams(
            collective_id=0, has_side_effects=True, vmem_limit_bytes=60 * 1024 * 1024
        ),
    )(
        pool_input,
        stream_in,
        group_weight,
        pool_scale[None, :],
        out_weight,
        norm_gain[None, :],
        table,
        expert_gate,
        expert_up,
        expert_down,
    )


def solution(mesh):
    placed = (
        P(("sp", "tp"), None),
        P(("sp", "tp"), None),
        P(),
        P(),
        P(),
        P(),
        P(("sp", "tp"), None),
        P(("sp", "tp"), None),
        P(("sp", "tp"), None, None),
        P(("sp", "tp"), None, None),
        P(("sp", "tp"), None, None),
    )
    return jax.shard_map(
        body, mesh=mesh, in_specs=placed, out_specs=P(("sp", "tp"), None), check_vma=False
    )
```

time: 128 us -> 118 us (0.922)
  the two profiles are of different devices: /device:TPU:13 before, /device:TPU:0 now
where the time goes in v2:
time: 118 us; the launch traced here: 117 us
  Pallas kernels  112 us (95%)
  local copies, waits for them, and re-layouts  3.02 us (3%)
  other arithmetic  2.29 us (2%)
    pallas_call x1, Pallas kernels, body(): pl.pallas_call(functools.partial(kernel, n, tp_size, main, extra), out_sh...  112 us

profile of v2, /device:TPU:0, one launch (start us, length us, event | category | flops | bytes accessed | tf_op | source)
XLA Modules:
  0.0 117.1 jit_solution(9879279203011444714)
XLA Ops:
  0.0 0.1 pad.2.clone
  0.1 0.8 eq.17
  0.8 0.2 convert_reduce_fusion
  1.1 0.1 reduce_sum.12
  1.2 0.7 fusion.2
  1.9 1.4 %maximum_maximum_fusion.table_ref = f32[8,192]{1,0:T(8,128)} fusion(f32[2,192]{1,0:T(2,128)} %bitcast.8, f32[2,192]{1,0:T(2,128)S(1)} %fusion.2, f32[8]{0:T(128)S(1)} %pad.2.clone), kind=kLoop, calls=%fused_computation.3 | loop fusion | flops 3072 | bytes 9248 | tf_op jit(solution)/shard_map/concatenate | solution.py:396
  3.2 111.8 %shard_map.109 = bf16[192,2048]{1,0:T(8,128)(2,1)} custom-call(bf16[192,1024]{1,0:T(8,128)(2,1)} %pool_hbm.1, bf16[192,2048]{1,0:T(8,128)(2,1)} %stream_hbm.1, bf16[4,256,256]{2,1,0:T(8,128)(2,1)} %group_hbm.1, f32[1,1024]{1,0:T(1,128)} %bitcast.7, bf16[1024,2048]{1,0:T(8,128)(2,1)} %out_hbm.1, f32[1,2048]{1,0:T(1,128)} %bitcast.5, ...), custom_call_target="tpu_custom_call" | custom-call | tf_op jit(solution)/shard_map/pallas_call | solution.py:409
  115.0 2.1 %copy.13 = bf16[192,2048]{1,0:T(8,128)(2,1)} copy(bf16[192,2048]{1,0:T(8,128)(2,1)} %shard_map.109) | data formatting | bytes 1572864
  (1 shorter events, 0.0 us)
